TPU v7x, 256 devices: a 4x2x16 block of a 4x16x16 slice. The times are simulated.
256 devices in a mesh: grp: 2 (over y), ep: 32 (over z, core), tp: 4 (over x).
Axes of the slice: x: 4, y: 2, z: 16, core: 2. Of those that a mesh axis runs over, the one named last changes fastest.
The devices are a block of a 4x16x16 slice.
Arguments:
- x_in: bfloat16 [4096, 2048], P(('grp', 'ep')), parts along dimension 0, may hold values from -6 to 6
- state: float32 [4096, 96, 128], P(('grp', 'ep'), 'tp'), parts along dimension 0, may hold values from -6 to 6
- routes: int32 [4096, 2], P(('grp', 'ep')), parts along dimension 0, may hold values from 0 to 63, as said below
- w_in: bfloat16 [2048, 1536], P(None, 'tp'), may hold values from -0.125 to 0.125
- decay_rate: float32 [96, 64], P('tp'), may hold values from 0.01 to 1
- frequency: float32 [96, 64], P('tp'), may hold values from 0 to 192
- log_step: float32 [96], P('tp'), may hold values from -3 to 0
- b_in: float32 [96, 16, 128], P('tp'), may hold values from -1.5 to 1.5
- c_out: float32 [96, 16, 128], P('tp'), may hold values from -0.5 to 0.5
- skip: float32 [1536], P('tp'), may hold values from -3 to 3
- w_out: bfloat16 [1536, 2048], P('tp'), may hold values from -0.15625 to 0.15625
- gain_mix: float32 [2048], replicated, may hold values from 0.1 to 1.9
- w_group: bfloat16 [2048, 4], replicated, may hold values from -0.0625 to 0.0625
- w_expert: bfloat16 [2048, 64], replicated, may hold values from -0.0625 to 0.0625
- w_gate: bfloat16 [64, 2048, 1024], P('ep', None, 'tp'), may hold values from -0.125 to 0.125
- w_up: bfloat16 [64, 2048, 1024], P('ep', None, 'tp'), may hold values from -0.125 to 0.125
- w_down: bfloat16 [64, 1024, 2048], P('ep', 'tp'), may hold values from -3 to 3
- gain_moe: float32 [2048], replicated, may hold values from 0.1 to 1.9
Outputs:
- layer_out: bfloat16 [4096, 2048], P(('grp', 'ep')), parts along dimension 0
- new_state: float32 [4096, 96, 128], P(('grp', 'ep'), 'tp'), parts along dimension 0
There are 2 independent parts, one for each index of `grp`. A program takes and returns all parts, laid end to end along the dimension named above; an argument that names none is the same for every part. Nothing has to cross between parts.
Inputs may be any that keep to these rules, and one draw needn't show every extreme that they name: `routes`: each row names two different experts of one group of 16 consecutive expert numbers. Within the rows of one index of ep (aligned blocks of 64 rows) no expert is named by more than 4 rows, and in every block some expert is named by exactly 4 rows.
All inputs are finite; a program needn't handle non-finite values.
Results may differ from a plain program's by a relative error of at most 0.015.
Values may be sent and summed in bfloat16 or wider, within the bound.
A program may use at most 64 MiB of HBM per device.

v0:
```python
import jax
import jax.numpy as jnp
from jax import lax
from jax.sharding import PartitionSpec as P

residual_scale = 8.0**0.25
norm_eps = 1e-05


def sent_to_all(x, axis):
    devices = lax.axis_size(axis)
    return lax.all_to_all(jnp.broadcast_to(x[None], (devices, *x.shape)), axis, 0, 0, tiled=True)


def taken_together(x, axis):
    everything = sent_to_all(x, axis)
    return jnp.sum(everything.astype(jnp.float32), axis=0)


def in_order(parts, dim):
    lengths = list(parts.shape[1:])
    lengths[dim] *= parts.shape[0]
    return jnp.moveaxis(parts, 0, dim).reshape(lengths)


def gather_directly(x, axis, dim):
    parts = sent_to_all(x, axis)
    return in_order(parts, dim)


def split_up(x, dim, devices):
    before, after = (x.shape[:dim], x.shape[dim + 1 :])
    return jnp.moveaxis(x.reshape(*before, devices, -1, *after), dim, 0)


def sent_and_summed(x, axis, dim):
    devices = lax.axis_size(axis)
    parts = lax.all_to_all(split_up(x, dim, devices), axis, 0, 0, tiled=True)
    return jnp.sum(parts.astype(jnp.float32), axis=0)


def normalize(values, gain):
    centre = jnp.mean(values, -1, keepdims=True)
    spread = jnp.mean(jnp.square(values - centre), -1, keepdims=True)
    return (values - centre) * lax.rsqrt(spread + norm_eps) * gain


def s5_advance(mix_input, state, decay_rate, frequency, log_step, b_in, c_out, skip):
    top_precision = lax.Precision.DEFAULT
    entries = decay_rate.shape[-1]
    group_count = decay_rate.shape[0]
    width = b_in.shape[1]
    seq_count = mix_input.shape[0]
    input_rows = mix_input.astype(jnp.float32).reshape(seq_count, group_count, width)
    step_size = jnp.exp(log_step)[:, None]
    lam_real = -decay_rate
    magnitude = jnp.exp(lam_real * step_size)
    angle_dt = frequency * step_size
    bar_real = magnitude * jnp.cos(angle_dt)
    bar_imag = magnitude * jnp.sin(angle_dt)
    minus_real = bar_real - 1.0
    modulus = lam_real * lam_real + frequency * frequency
    ratio_real = (minus_real * lam_real + bar_imag * frequency) / modulus
    ratio_imag = (bar_imag * lam_real - minus_real * frequency) / modulus
    in_real = b_in[..., :entries]
    in_imag = b_in[..., entries:]
    input_matrix_real = ratio_real[:, None, :] * in_real - ratio_imag[:, None, :] * in_imag
    input_matrix_imag = ratio_real[:, None, :] * in_imag + ratio_imag[:, None, :] * in_real
    forcing_real = jnp.einsum(
        "rxf,xfb->rxb", input_rows, input_matrix_real, precision=top_precision
    )
    forcing_imag = jnp.einsum(
        "rxf,xfb->rxb", input_rows, input_matrix_imag, precision=top_precision
    )
    old_real = state[..., :entries]
    old_imag = state[..., entries:]
    following_real = bar_real * old_real - bar_imag * old_imag + forcing_real
    following_imag = bar_real * old_imag + bar_imag * old_real + forcing_imag
    output_real = c_out[..., :entries]
    output_imag = c_out[..., entries:]
    output_matrix = jnp.einsum("lzt,zft->lzf", following_real, output_real, precision=top_precision)
    output_matrix = output_matrix - jnp.einsum(
        "lzt,zft->lzf", following_imag, output_imag, precision=top_precision
    )
    output_matrix = output_matrix + skip.reshape(group_count, width) * input_rows
    activated = jax.nn.gelu(output_matrix).reshape(seq_count, group_count * width)
    return (activated, jnp.concatenate([following_real, following_imag], axis=-1))


def route_weights(normed, routes, w_group, w_expert):
    group_total = w_group.shape[1]
    expert_total = w_expert.shape[1]
    per_group = expert_total // group_total
    group_logit = jnp.dot(normed, w_group, preferred_element_type=jnp.float32)
    group_exp = jnp.exp(group_logit)
    group_prob = group_exp / jnp.sum(group_exp, -1, keepdims=True)
    chosen = routes[:, 0] // per_group
    group_pick = jnp.sum(
        jnp.where(
            chosen[:, None] == jnp.arange(group_total, dtype=jnp.int32)[None, :], group_prob, 0.0
        ),
        -1,
    )
    expert_logit = jnp.dot(normed, w_expert, preferred_element_type=jnp.float32)
    picked = jnp.sum(
        jnp.where(
            routes[:, :, None] == jnp.arange(expert_total, dtype=jnp.int32)[None, None, :],
            expert_logit[:, None, :],
            0.0,
        ),
        -1,
    )
    pair_exp = jnp.exp(picked)
    return pair_exp / jnp.sum(pair_exp, -1, keepdims=True) * group_pick[:, None]


def per_device(
    x_in,
    state,
    routes,
    w_in,
    decay_rate,
    frequency,
    log_step,
    b_in,
    c_out,
    skip,
    w_out,
    gain_mix,
    w_group,
    w_expert,
    w_gate,
    w_up,
    w_down,
    gain_moe,
):
    top_precision = lax.Precision.DEFAULT
    seq_count = x_in.shape[0]
    model_width = x_in.shape[1]
    mix_input = jnp.dot(x_in, w_in, preferred_element_type=jnp.float32).astype(jnp.bfloat16)
    activated, new_state = s5_advance(
        mix_input, state, decay_rate, frequency, log_step, b_in, c_out, skip
    )
    partial_mix = jnp.dot(activated.astype(jnp.bfloat16), w_out, preferred_element_type=jnp.float32)
    mixed = taken_together(partial_mix.astype(jnp.bfloat16), "tp").astype(jnp.float32)
    hidden_state = normalize(residual_scale * x_in.astype(jnp.float32) + mixed, gain_mix)
    hidden_bf = hidden_state.astype(jnp.bfloat16)
    route_weight = route_weights(hidden_bf, routes, w_group, w_expert)
    expert_total = w_expert.shape[1]
    ep_count = lax.axis_size("ep")
    local_experts = w_gate.shape[0]
    capacity = max(2, 4 * seq_count // expert_total)
    total_slots = expert_total * capacity
    hits = (routes[:, :, None] == jnp.arange(expert_total, dtype=jnp.int32)[None, None, :]).astype(
        jnp.int32
    )
    tally = jnp.sum(hits, axis=1)
    prior = jnp.cumsum(tally, axis=0) - tally
    slot_in_block = jnp.sum(prior[:, None, :] * hits, axis=-1)
    target = routes * capacity + slot_in_block
    slot_ids = jnp.arange(total_slots, dtype=jnp.int32)
    matches = target[:, :, None] == slot_ids[None, None, :]
    dispatch_map = jnp.any(slot_ids[:, None, None] == target[None, :, :], axis=-1).astype(
        jnp.bfloat16
    )
    combine_map = jnp.sum(jnp.where(matches, route_weight[:, :, None], 0.0), axis=1)
    buffer = jnp.dot(dispatch_map, hidden_bf, preferred_element_type=jnp.float32).astype(
        jnp.bfloat16
    )
    buffer = buffer.reshape(ep_count, local_experts, capacity, model_width)
    column_width = model_width // lax.axis_size("tp")
    own_columns = lax.dynamic_slice_in_dim(
        buffer, lax.axis_index("tp") * column_width, column_width, 3
    )
    piece = gather_directly(
        lax.all_to_all(own_columns, "ep", split_axis=0, concat_axis=0, tiled=True), "tp", 3
    )
    gate_part = jnp.einsum("njcd,jdf->njcf", piece, w_gate, preferred_element_type=jnp.float32)
    up_part = jnp.einsum("njcd,jdf->njcf", piece, w_up, preferred_element_type=jnp.float32)
    act = (jax.nn.silu(gate_part) * up_part).astype(jnp.bfloat16)
    share = sent_and_summed(
        jnp.einsum("njcf,jfd->njcd", act, w_down, preferred_element_type=jnp.float32).astype(
            jnp.bfloat16
        ),
        "tp",
        3,
    ).astype(jnp.bfloat16)
    returned_rows = lax.all_to_all(share, "ep", split_axis=0, concat_axis=0, tiled=True)
    flat_rows = returned_rows.reshape(total_slots, returned_rows.shape[3])
    moe = jnp.dot(
        combine_map,
        lax.all_gather(flat_rows, "tp", axis=1, tiled=True).astype(jnp.float32),
        precision=top_precision,
    )
    layer_out = normalize(residual_scale * hidden_state + moe, gain_moe).astype(jnp.bfloat16)
    return (layer_out, new_state)


def solution(mesh):
    in_specs = (
        P(("grp", "ep"), None),
        P(("grp", "ep"), "tp", None),
        P(("grp", "ep"), None),
        P(None, "tp"),
        P("tp", None),
        P("tp", None),
        P("tp"),
        P("tp", None, None),
        P("tp", None, None),
        P("tp"),
        P("tp", None),
        P(),
        P(),
        P(),
        P("ep", None, "tp"),
        P("ep", None, "tp"),
        P("ep", "tp", None),
        P(),
    )
    out_specs = (P(("grp", "ep"), None), P(("grp", "ep"), "tp", None))
    return jax.shard_map(
        per_device, mesh=mesh, in_specs=in_specs, out_specs=out_specs, check_vma=False
    )
```

profile of v0, /device:TPU:40, one launch (start us, length us, event | category | flops | bytes accessed | tf_op | source)
XLA Modules:
  0.0 197.4 jit_solution(56538877208457532)
XLA Ops:
  8.0 1.9 convolution_convert_fusion.3
  11.4 1.4 fusion.6
  12.9 1.6 fusion.41
  15.3 1.2 broadcast_in_dim.24
  16.4 4.6 %all-to-all-start = ((bf16[4,64,2048]{2,1,0:T(8,128)(2,1)}), bf16[4,64,2048]{2,1,0:T(8,128)(2,1)}, u32[]{:S(2)}, u32[]{:S(2)}) async-start(bf16[4,64,2048]{2,1,0:T(8,128)(2,1)} %broadcast_in_dim.24), calls=%async_computation | async-start | bytes 2097152 | tf_op jit(solution)/shard_map/all_to_all | solution.py:12
  21.5 14.8 %all-to-all-done = bf16[4,64,2048]{2,1,0:T(8,128)(2,1)} async-done(((bf16[4,64,2048]{2,1,0:T(8,128)(2,1)}), bf16[4,64,2048]{2,1,0:T(8,128)(2,1)}, u32[]{:S(2)}, u32[]{:S(2)}) %all-to-all-start) | async-done | bytes 1048608 | tf_op jit(solution)/shard_map/all_to_all | solution.py:12
  36.3 1.4 convert_reduce_fusion
  38.8 1.2 multiply_reduce_fusion.1
  41.8 1.5 convolution_convert_fusion.1
  43.3 2.3 %reshape.109 = bf16[32,2,4,2048]{3,2,1,0:T(4,128)(2,1)} reshape(bf16[256,2048]{1,0:T(8,128)(2,1)} %convolution_convert_fusion.1) | data formatting | bytes 2097152 | tf_op jit(solution)/shard_map/reshape | solution.py:170
  46.6 46.5 %all_to_all.25 = bf16[32,2,4,512]{3,2,1,0:T(4,128)(2,1)S(1)} all-to-all(bf16[32,2,4,512]{3,2,1,0:T(4,128)(2,1)S(1)} %constant_dynamic-slice_fusion), channel_id=1, replica_groups=mesh['grp'=2,'ep'=32,'tp'=4] {'ep'}, dimensions={0} | all-to-all | bytes 524288 | tf_op jit(solution)/shard_map/all_to_all | solution.py:176
  93.4 18.0 %all_to_all.26 = bf16[4,32,2,4,512]{4,1,3,2,0:T(8,128)(2,1)S(1)} all-to-all(bf16[4,32,2,4,512]{4,1,3,2,0:T(8,128)(2,1)S(1)} %broadcast_in_dim.34), channel_id=1, replica_groups=mesh['grp'=2,'ep'=32,'tp'=4] {'tp'}, dimensions={0} | all-to-all | bytes 2097152 | tf_op jit(solution)/shard_map/all_to_all | solution.py:12
  112.6 1.2 fusion.7
  113.7 3.8 %convolution_convert_fusion = bf16[2,32,4,2048]{3,1,2,0:T(8,128)(2,1)} fusion(bf16[2,256,2048]{2,1,0:T(8,128)(2,1)S(1)} %copy-done, bf16[32,2,4,2048]{3,0,2,1:T(8,128)(2,1)} %bitcast.85, bf16[2,2048,256]{2,1,0:T(8,128)(2,1)} %param.33, f32[32,2,4,256]{3,0,2,1:T(8,128)} %fusion.7), kind=kOutput, calls=%fused_computation | convolution fusion | flops 537788416 | bytes 6553600 | tf_op jit(solution)/shard_map/njcf,jfd->njcd/dot_general | solution.py:182
  117.5 1.4 copy.95
  118.8 17.5 %all_to_all.27 = bf16[4,32,2,4,512]{4,1,3,2,0:T(8,128)(2,1)} all-to-all(bf16[4,32,2,4,512]{4,1,3,2,0:T(8,128)(2,1)S(1)} %bitcast.88), channel_id=1, replica_groups=mesh['grp'=2,'ep'=32,'tp'=4] {'tp'}, dimensions={0} | all-to-all | bytes 2097152 | tf_op jit(solution)/shard_map/all_to_all | solution.py:38
  136.3 2.2 %reduce_sum.130 = bf16[32,2,4,512]{3,0,2,1:T(8,128)(2,1)} reduce(bf16[4,32,2,4,512]{4,1,3,2,0:T(8,128)(2,1)} %all_to_all.27, bf16[]{:T(256)} %constant.58.clone.1), dimensions={0}, to_apply=%region_12.13 | reduce | flops 393216 | bytes 1310722 | tf_op jit(solution)/shard_map/reduce_sum | solution.py:39
  138.5 1.2 copy.80
  139.7 26.5 %all_to_all.28 = bf16[32,2,4,512]{3,2,1,0:T(4,128)(2,1)} all-to-all(bf16[32,2,4,512]{3,2,1,0:T(4,128)(2,1)S(1)} %copy.80), channel_id=1, replica_groups=mesh['grp'=2,'ep'=32,'tp'=4] {'ep'}, dimensions={0} | all-to-all | bytes 524288 | tf_op jit(solution)/shard_map/all_to_all | solution.py:188
  166.2 1.7 reshape.112
  168.0 1.5 pad_maximum_fusion
  169.5 1.3 copy.81
  171.7 16.1 %all-gather.2.cloned.1.call-done = bf16[256,2048]{1,0:T(8,128)(2,1)} async-done(((bf16[256,512]{1,0:T(8,128)(2,1)}), bf16[256,2048]{1,0:T(8,128)(2,1)}) %all-gather.2.cloned.1.call-update) | async-done | bytes 1048592 | tf_op jit(solution)/shard_map/all_gather | solution.py:192
  187.8 1.7 fusion.62
  (72 shorter events, 10.8 us)
Async XLA Ops:
  7.2 106.6 %copy-start = (bf16[2,256,2048]{2,1,0:T(8,128)(2,1)S(1)}, bf16[2,256,2048]{2,1,0:T(8,128)(2,1)}, u32[]{:S(2)}) copy-start(bf16[2,256,2048]{2,1,0:T(8,128)(2,1)} %param.34) | copy-start | bytes 6291460
  7.2 2.9 %copy-start.5 = (f32[64,24,128]{2,1,0:T(8,128)S(1)}, f32[64,24,128]{2,1,0:T(8,128)}, u32[]{:S(2)}) copy-start(f32[64,24,128]{2,1,0:T(8,128)} %param.19) | copy-start | bytes 2359300
  9.9 0.7 copy-start.14
  9.9 0.7 copy-start.15
  9.9 0.9 copy-start.9
  10.9 1.9 copy-start.17
  10.9 2.0 %copy-start.8 = (f32[24,16,128]{2,1,0:T(8,128)S(1)}, f32[24,16,128]{2,1,0:T(8,128)}, u32[]{:S(2)}) copy-start(f32[24,16,128]{2,1,0:T(8,128)} %param.26) | copy-start | bytes 589828
  12.9 2.0 %copy-start.7 = (bf16[384,2048]{1,0:T(8,128)(2,1)S(1)}, bf16[384,2048]{1,0:T(8,128)(2,1)}, u32[]{:S(2)}) copy-start(bf16[384,2048]{1,0:T(8,128)(2,1)} %param.28) | copy-start | bytes 4718596
  15.3 5.8 %copy-start.13 = (s32[64,2]{0,1:T(2,128)S(1)}, s32[64,2]{0,1:T(2,128)}, u32[]{:S(2)}) copy-start(s32[64,2]{0,1:T(2,128)} %param.20) | copy-start | bytes 1540
  16.4 19.8 %all-to-all-start = ((bf16[4,64,2048]{2,1,0:T(8,128)(2,1)}), bf16[4,64,2048]{2,1,0:T(8,128)(2,1)}, u32[]{:S(2)}, u32[]{:S(2)}) async-start(bf16[4,64,2048]{2,1,0:T(8,128)(2,1)} %broadcast_in_dim.24), calls=%async_computation | async-start | bytes 2097152 | tf_op jit(solution)/shard_map/all_to_all | solution.py:12
  21.0 19.0 %copy-start.11 = (f32[2048]{0:T(1024)S(1)}, f32[2048]{0:T(1024)}, u32[]{:S(2)}) copy-start(f32[2048]{0:T(1024)} %param.29) | copy-start | bytes 24580
  21.0 166.7 %all-gather.2.cloned.1.call-start = ((), (), s32[]{:S(2)}) async-start(), calls=%async_computation.5 | async-start | bytes 1310720 | tf_op jit(solution)/shard_map/all_gather | solution.py:192
  41.1 0.7 copy-start.3
  93.4 19.2 %copy-start.6 = (bf16[2,2048,256]{2,1,0:T(8,128)(2,1)S(1)}, bf16[2,2048,256]{2,1,0:T(8,128)(2,1)}, u32[]{:S(2)}) copy-start(bf16[2,2048,256]{2,1,0:T(8,128)(2,1)} %param.32) | copy-start | bytes 6291460
  111.6 1.0 copy-start.1
  168.0 2.9 %copy-start.4 = (bf16[64,2048]{1,0:T(8,128)(2,1)S(1)}, bf16[64,2048]{1,0:T(8,128)(2,1)}, u32[]{:S(2)}) copy-start(bf16[64,2048]{1,0:T(8,128)(2,1)} %copy-done.3) | copy-start | bytes 786436
  168.0 2.9 %copy-start.10 = (bf16[2048,64]{0,1:T(8,128)(2,1)S(1)}, bf16[2048,64]{0,1:T(8,128)(2,1)}, u32[]{:S(2)}) copy-start(bf16[2048,64]{0,1:T(8,128)(2,1)} %param.31) | copy-start | bytes 786436
  168.0 3.3 %copy-start.12 = (bf16[2048,4]{0,1:T(4,128)(2,1)S(1)}, bf16[2048,4]{0,1:T(4,128)(2,1)}, u32[]{:S(2)}) copy-start(bf16[2048,4]{0,1:T(4,128)(2,1)} %param.30) | copy-start | bytes 49156
  169.5 18.3 %copy-start.2 = (bf16[64,2048]{1,0:T(8,128)(2,1)S(1)}, bf16[64,2048]{1,0:T(8,128)(2,1)}, u32[]{:S(2)}) copy-start(bf16[64,2048]{1,0:T(8,128)(2,1)} %param.18) | copy-start | bytes 786436
  170.8 18.8 %copy-start.16 = (f32[2048]{0:T(1024)S(1)}, f32[2048]{0:T(1024)}, u32[]{:S(2)}) copy-start(f32[2048]{0:T(1024)} %param.35) | copy-start | bytes 24580
Sparse Core Ops, SparseCore 0:
  168.1 19.5 all-gather.1
where the time goes:
time: 198 us; the launch traced here: 197 us
  blocking collectives  109 us (55%)
  waiting for transfers between devices  30.9 us (16%)
  matrix products  14.6 us (7%)
  between operations  14.4 us (7%)
  local copies, waits for them, and re-layouts  13.8 us (7%)
  other arithmetic  10.5 us (5%)
  starting transfers between devices  4.58 us (2%)
    all_to_all x1, blocking collectives, per_device(): lax.all_to_all(own_columns, 'ep', split_axis=0, concat_axis=0, tiled=True)  46.5 us
    all_to_all x1, blocking collectives, per_device(): lax.all_to_all(share, 'ep', split_axis=0, concat_axis=0, tiled=True)  26.5 us
    all_to_all x1, blocking collectives, sent_to_all(): lax.all_to_all(jnp.broadcast_to(x[None], (devices, *x.shape)), axis, 0, 0...  18 us
    all_to_all x1, blocking collectives, sent_and_summed(): parts = lax.all_to_all(split_up(x, dim, devices), axis, 0, 0, tiled=True)  17.5 us
    all_gather x1, waiting for transfers between devices, per_device(): lax.all_gather(flat_rows, 'tp', axis=1, tiled=True).astype(jnp.float32)  16.1 us
    all_to_all x1, waiting for transfers between devices, sent_to_all(): lax.all_to_all(jnp.broadcast_to(x[None], (devices, *x.shape)), axis, 0, 0...  14.8 us
    all_to_all x1, starting transfers between devices, sent_to_all(): lax.all_to_all(jnp.broadcast_to(x[None], (devices, *x.shape)), axis, 0, 0...  4.58 us
  transfers between devices with their start and end apart: 2, of which 2 were waited for; matrix products, arithmetic and copies ran while one was open for 2% of the time, Pallas kernels for 0%

commit v1 on v0

--- a/solution.py
+++ b/solution.py
@@ -189,7 +189,7 @@
     flat_rows = returned_rows.reshape(total_slots, returned_rows.shape[3])
     moe = jnp.dot(
         combine_map,
-        lax.all_gather(flat_rows, "tp", axis=1, tiled=True).astype(jnp.float32),
+        jnp.concatenate(lax.all_gather(flat_rows, "tp"), axis=1).astype(jnp.float32),
         precision=top_precision,
     )
     layer_out = normalize(residual_scale * hidden_state + moe, gain_moe).astype(jnp.bfloat16)

time: 198 us -> 201 us (1.015)
  local copies, waits for them, and re-layouts: 13.8 us -> 16.1 us
    all_gather x0 -> x1, local copies, waits for them, and re-layouts: none -> 2.28 us  [per_device(): lax.all_gather(flat_rows, 'tp')]
where the time goes in v1:
time: 201 us; the launch traced here: 200 us
  blocking collectives  109 us (54%)
  waiting for transfers between devices  30.9 us (15%)
  local copies, waits for them, and re-layouts  16.1 us (8%)
  matrix products  14.7 us (7%)
  between operations  14.4 us (7%)
  other arithmetic  10.5 us (5%)
  starting transfers between devices  4.58 us (2%)
    all_to_all x1, blocking collectives, per_device(): lax.all_to_all(own_columns, 'ep', split_axis=0, concat_axis=0, tiled=True)  46.5 us
    all_to_all x1, blocking collectives, per_device(): lax.all_to_all(share, 'ep', split_axis=0, concat_axis=0, tiled=True)  26.5 us
    all_to_all x1, blocking collectives, sent_to_all(): lax.all_to_all(jnp.broadcast_to(x[None], (devices, *x.shape)), axis, 0, 0...  18 us
    all_to_all x1, blocking collectives, sent_and_summed(): parts = lax.all_to_all(split_up(x, dim, devices), axis, 0, 0, tiled=True)  17.5 us
    all_gather x1, waiting for transfers between devices, per_device(): lax.all_gather(flat_rows, 'tp')  16.1 us
    all_to_all x1, waiting for transfers between devices, sent_to_all(): lax.all_to_all(jnp.broadcast_to(x[None], (devices, *x.shape)), axis, 0, 0...  14.8 us
    all_to_all x1, starting transfers between devices, sent_to_all(): lax.all_to_all(jnp.broadcast_to(x[None], (devices, *x.shape)), axis, 0, 0...  4.58 us
  transfers between devices with their start and end apart: 2, of which 2 were waited for; matrix products, arithmetic and copies ran while one was open for 2% of the time, Pallas kernels for 0%

profile of v1, /device:TPU:40, one launch (start us, length us, event | category | flops | bytes accessed | tf_op | source)
XLA Modules:
  0.0 199.8 jit_solution(11680402529090747527)
XLA Ops:
  8.0 1.9 convolution_convert_fusion.3
  11.4 1.4 fusion.6
  12.9 1.6 fusion.41
  15.3 1.2 broadcast_in_dim.24
  16.4 4.6 %all-to-all-start = ((bf16[4,64,2048]{2,1,0:T(8,128)(2,1)}), bf16[4,64,2048]{2,1,0:T(8,128)(2,1)}, u32[]{:S(2)}, u32[]{:S(2)}) async-start(bf16[4,64,2048]{2,1,0:T(8,128)(2,1)} %broadcast_in_dim.24), calls=%async_computation | async-start | bytes 2097152 | tf_op jit(solution)/shard_map/all_to_all | solution.py:12
  21.5 14.8 %all-to-all-done = bf16[4,64,2048]{2,1,0:T(8,128)(2,1)} async-done(((bf16[4,64,2048]{2,1,0:T(8,128)(2,1)}), bf16[4,64,2048]{2,1,0:T(8,128)(2,1)}, u32[]{:S(2)}, u32[]{:S(2)}) %all-to-all-start) | async-done | bytes 1048608 | tf_op jit(solution)/shard_map/all_to_all | solution.py:12
  36.3 1.4 convert_reduce_fusion
  38.8 1.2 multiply_reduce_fusion.1
  41.8 1.5 convolution_convert_fusion.1
  43.3 2.3 %reshape.112 = bf16[32,2,4,2048]{3,2,1,0:T(4,128)(2,1)} reshape(bf16[256,2048]{1,0:T(8,128)(2,1)} %convolution_convert_fusion.1) | data formatting | bytes 2097152 | tf_op jit(solution)/shard_map/reshape | solution.py:170
  46.6 46.5 %all_to_all.25 = bf16[32,2,4,512]{3,2,1,0:T(4,128)(2,1)S(1)} all-to-all(bf16[32,2,4,512]{3,2,1,0:T(4,128)(2,1)S(1)} %constant_dynamic-slice_fusion), channel_id=1, replica_groups=mesh['grp'=2,'ep'=32,'tp'=4] {'ep'}, dimensions={0} | all-to-all | bytes 524288 | tf_op jit(solution)/shard_map/all_to_all | solution.py:176
  93.4 18.0 %all_to_all.26 = bf16[4,32,2,4,512]{4,1,3,2,0:T(8,128)(2,1)S(1)} all-to-all(bf16[4,32,2,4,512]{4,1,3,2,0:T(8,128)(2,1)S(1)} %broadcast_in_dim.34), channel_id=1, replica_groups=mesh['grp'=2,'ep'=32,'tp'=4] {'tp'}, dimensions={0} | all-to-all | bytes 2097152 | tf_op jit(solution)/shard_map/all_to_all | solution.py:12
  112.6 1.2 fusion.7
  113.7 3.8 %convolution_convert_fusion = bf16[2,32,4,2048]{3,1,2,0:T(8,128)(2,1)} fusion(bf16[2,256,2048]{2,1,0:T(8,128)(2,1)S(1)} %copy-done, bf16[32,2,4,2048]{3,0,2,1:T(8,128)(2,1)} %bitcast.88, bf16[2,2048,256]{2,1,0:T(8,128)(2,1)} %param.33, f32[32,2,4,256]{3,0,2,1:T(8,128)} %fusion.7), kind=kOutput, calls=%fused_computation | convolution fusion | flops 537788416 | bytes 6553600 | tf_op jit(solution)/shard_map/njcf,jfd->njcd/dot_general | solution.py:182
  117.5 1.4 copy.96
  118.8 17.5 %all_to_all.27 = bf16[4,32,2,4,512]{4,1,3,2,0:T(8,128)(2,1)} all-to-all(bf16[4,32,2,4,512]{4,1,3,2,0:T(8,128)(2,1)S(1)} %bitcast.92), channel_id=1, replica_groups=mesh['grp'=2,'ep'=32,'tp'=4] {'tp'}, dimensions={0} | all-to-all | bytes 2097152 | tf_op jit(solution)/shard_map/all_to_all | solution.py:38
  136.3 2.2 %reduce_sum.130 = bf16[32,2,4,512]{3,0,2,1:T(8,128)(2,1)} reduce(bf16[4,32,2,4,512]{4,1,3,2,0:T(8,128)(2,1)} %all_to_all.27, bf16[]{:T(256)} %constant.58.clone.1), dimensions={0}, to_apply=%region_12.13 | reduce | flops 393216 | bytes 1310722 | tf_op jit(solution)/shard_map/reduce_sum | solution.py:39
  139.7 26.5 %all_to_all.28 = bf16[32,2,4,512]{3,2,1,0:T(4,128)(2,1)} all-to-all(bf16[32,2,4,512]{3,2,1,0:T(4,128)(2,1)S(1)} %copy.80), channel_id=1, replica_groups=mesh['grp'=2,'ep'=32,'tp'=4] {'ep'}, dimensions={0} | all-to-all | bytes 524288 | tf_op jit(solution)/shard_map/all_to_all | solution.py:188
  166.2 1.7 all_gather_reshape.3
  168.0 1.5 pad_maximum_fusion
  169.5 1.3 copy.82
  171.7 16.1 %all-gather.2.cloned.1.call-done = bf16[4,256,512]{2,1,0:T(8,128)(2,1)} async-done(((bf16[1,256,512]{2,1,0:T(8,128)(2,1)}), bf16[4,256,512]{2,1,0:T(8,128)(2,1)}) %all-gather.2.cloned.1.call-update) | async-done | bytes 1048592 | tf_op jit(solution)/shard_map/all_gather | solution.py:192
  187.8 2.3 %copy.81 = bf16[4,256,512]{1,2,0:T(8,128)(2,1)} copy(bf16[4,256,512]{2,1,0:T(8,128)(2,1)} %all-gather.2.cloned.1.call-done) | data formatting | bytes 2097152 | tf_op jit(solution)/shard_map/all_gather | solution.py:192
  190.0 1.8 fusion.62
  (73 shorter events, 12.0 us)
Async XLA Ops:
  7.2 106.6 %copy-start = (bf16[2,256,2048]{2,1,0:T(8,128)(2,1)S(1)}, bf16[2,256,2048]{2,1,0:T(8,128)(2,1)}, u32[]{:S(2)}) copy-start(bf16[2,256,2048]{2,1,0:T(8,128)(2,1)} %param.34) | copy-start | bytes 6291460
  7.2 2.9 %copy-start.5 = (f32[64,24,128]{2,1,0:T(8,128)S(1)}, f32[64,24,128]{2,1,0:T(8,128)}, u32[]{:S(2)}) copy-start(f32[64,24,128]{2,1,0:T(8,128)} %param.19) | copy-start | bytes 2359300
  9.9 0.7 copy-start.14
  9.9 0.7 copy-start.15
  9.9 0.9 copy-start.9
  10.9 1.9 copy-start.17
  10.9 2.0 copy-start.8
  12.9 2.0 copy-start.7
  15.3 5.8 %copy-start.13 = (s32[64,2]{0,1:T(2,128)S(1)}, s32[64,2]{0,1:T(2,128)}, u32[]{:S(2)}) copy-start(s32[64,2]{0,1:T(2,128)} %param.20) | copy-start | bytes 1540
  16.4 19.8 %all-to-all-start = ((bf16[4,64,2048]{2,1,0:T(8,128)(2,1)}), bf16[4,64,2048]{2,1,0:T(8,128)(2,1)}, u32[]{:S(2)}, u32[]{:S(2)}) async-start(bf16[4,64,2048]{2,1,0:T(8,128)(2,1)} %broadcast_in_dim.24), calls=%async_computation | async-start | bytes 2097152 | tf_op jit(solution)/shard_map/all_to_all | solution.py:12
  21.0 19.0 %copy-start.11 = (f32[2048]{0:T(1024)S(1)}, f32[2048]{0:T(1024)}, u32[]{:S(2)}) copy-start(f32[2048]{0:T(1024)} %param.29) | copy-start | bytes 24580
  21.0 166.8 %all-gather.2.cloned.1.call-start = ((), (), s32[]{:S(2)}) async-start(), calls=%async_computation.5 | async-start | bytes 1310720 | tf_op jit(solution)/shard_map/all_gather | solution.py:192
  41.1 0.7 copy-start.3
  93.4 19.2 %copy-start.6 = (bf16[2,2048,256]{2,1,0:T(8,128)(2,1)S(1)}, bf16[2,2048,256]{2,1,0:T(8,128)(2,1)}, u32[]{:S(2)}) copy-start(bf16[2,2048,256]{2,1,0:T(8,128)(2,1)} %param.32) | copy-start | bytes 6291460
  111.6 1.0 copy-start.1
  168.0 2.9 %copy-start.4 = (bf16[64,2048]{1,0:T(8,128)(2,1)S(1)}, bf16[64,2048]{1,0:T(8,128)(2,1)}, u32[]{:S(2)}) copy-start(bf16[64,2048]{1,0:T(8,128)(2,1)} %copy-done.3) | copy-start | bytes 786436
  168.0 2.9 %copy-start.10 = (bf16[2048,64]{0,1:T(8,128)(2,1)S(1)}, bf16[2048,64]{0,1:T(8,128)(2,1)}, u32[]{:S(2)}) copy-start(bf16[2048,64]{0,1:T(8,128)(2,1)} %param.31) | copy-start | bytes 786436
  168.0 3.3 %copy-start.12 = (bf16[2048,4]{0,1:T(4,128)(2,1)S(1)}, bf16[2048,4]{0,1:T(4,128)(2,1)}, u32[]{:S(2)}) copy-start(bf16[2048,4]{0,1:T(4,128)(2,1)} %param.30) | copy-start | bytes 49156
  169.5 20.6 %copy-start.2 = (bf16[64,2048]{1,0:T(8,128)(2,1)S(1)}, bf16[64,2048]{1,0:T(8,128)(2,1)}, u32[]{:S(2)}) copy-start(bf16[64,2048]{1,0:T(8,128)(2,1)} %param.18) | copy-start | bytes 786436
  171.6 20.4 %copy-start.16 = (f32[2048]{0:T(1024)S(1)}, f32[2048]{0:T(1024)}, u32[]{:S(2)}) copy-start(f32[2048]{0:T(1024)} %param.35) | copy-start | bytes 24580
Sparse Core Ops, SparseCore 0:
  168.1 19.6 all-gather.1
